TPU v7x, 256 devices: a whole 4x4x8 slice. The times are simulated.
256 devices in a mesh: sp: 32 (over z, x), fs: 4 (over y), tp: 2 (over core).
Axes of the slice: x: 4, y: 4, z: 8, core: 2. Of those that a mesh axis runs over, the one named last changes fastest.
Arguments:
- tokens: bfloat16 [4, 8192, 2048], P('fs', 'sp', 'tp'), may hold values from -6 to 6
- norm_gain: float32 [2048], replicated, may hold values from 0.1 to 1.9
- query_weight: bfloat16 [2048, 1024], P(('sp', 'fs'), 'tp'), may hold values from -0.125 to 0.125
- forget_weight: bfloat16 [2048, 1024], P(('sp', 'fs'), 'tp'), may hold values from -0.125 to 0.125
- value_weight: bfloat16 [2048, 1024], P(('sp', 'fs'), 'tp'), may hold values from -0.125 to 0.125
- outgate_weight: bfloat16 [2048, 1024], P(('sp', 'fs'), 'tp'), may hold values from -0.125 to 0.125
- pool_in_weight: bfloat16 [2048, 1024], P(('sp', 'fs'), 'tp'), may hold values from -0.125 to 0.125
- forget_room: float32 [1024], P('tp'), may hold values from 0 to 0.06
- decay_shift: float32 [4, 8192, 8], P('fs', 'sp', 'tp'), may hold values from -0.6 to 0
- head_gain: float32 [128], replicated, may hold values from 0.1 to 1.9
- start_state: float32 [4, 8, 128, 128], P('fs', 'tp'), may hold values from -0.03314563 to 0.03314563
- pool_map: bfloat16 [4, 256, 256], P('tp'), may hold values from -0.375 to 0.375
- pool_scale: float32 [1024], P('tp'), may hold values from 0.1 to 1.9
- out_rec_weight: bfloat16 [1024, 2048], P('tp', ('sp', 'fs')), may hold values from -0.125 to 0.125
- out_pool_weight: bfloat16 [1024, 2048], P('tp', ('sp', 'fs')), may hold values from -0.125 to 0.125
Outputs:
- mixed: bfloat16 [4, 8192, 2048], P('fs', ('sp', 'tp'))
All inputs are finite; a program needn't handle non-finite values.
Results may differ from a plain program's by a relative error of at most 0.013.
Values may be sent and summed in bfloat16 or wider, within the bound.
A program may use at most 128 MiB of HBM per device.

v0:
```python
import jax
import jax.numpy as jnp
from jax import lax
from jax.sharding import Mesh
from jax.sharding import PartitionSpec as P

HEAD = 128
POOL_DIM = 256
WIDEST = 16
BLOCK = 128
SP_FS = ("sp_0", "sp_1", "fs")
SP = ("sp_0", "sp_1")
SP_TP = ("sp_0", "sp_1", "tp")
EPSILON = 1e-06


def from_everyone(array, axis):
    count = lax.axis_size(axis)
    return lax.all_to_all(
        jnp.broadcast_to(array[None], (count, *array.shape)), axis, 0, 0, tiled=True
    )


def laid_out(blocks, dim):
    blocks = jnp.moveaxis(blocks, 0, dim)
    lengths = blocks.shape
    return blocks.reshape(*lengths[:dim], lengths[dim] * lengths[dim + 1], *lengths[dim + 2 :])


def gather_directly(array, axis, dim):
    blocks = from_everyone(array, axis)
    return laid_out(blocks, dim)


def gather_turned(arrays, axis, dims):
    turned = [jnp.moveaxis(a, dim, 0) for a, dim in zip(arrays, dims)]
    both = jnp.concatenate([t.reshape(len(t), -1) for t in turned], axis=1)
    filled, at, done = (lax.all_gather(both, axis, axis=0, tiled=True), 0, [])
    for t, dim in zip(turned, dims):
        slab = filled[:, at : at + t[0].size].reshape(-1, *t.shape[1:])
        done.append(jnp.moveaxis(slab, 0, dim))
        at += t[0].size
    return tuple(done)


def neutral_like(array, identity):
    return jax.tree.map(
        lambda part, zero: jnp.zeros_like(part) + jnp.asarray(zero, part.dtype), array, identity
    )


def entering_2(array, axes, combine, identity):
    before = start = neutral_like(array, identity)
    so_far = array
    for axis in reversed(axes):
        count, mine = (lax.axis_size(axis), lax.axis_index(axis))
        pieces = jax.tree.map(
            lambda part, kind: lax.all_gather(part.astype(kind), axis),
            so_far,
            (jnp.bfloat16, jnp.bfloat16),
        )
        inside, so_far = (start, start)
        for k in range(count):
            passed = k < mine
            so_far = combine(
                so_far, jax.tree.map(lambda part, own: part[k].astype(own.dtype), pieces, array)
            )
            inside = jax.tree.map(lambda new, old: jnp.where(passed, new, old), so_far, inside)
        before = combine(inside, before)
    return before


def shifted(value, axis, steps):
    count = lax.axis_size(axis)
    first, last = (max(0, -steps), min(count, count - steps))
    return lax.ppermute(value, axis, [(source, source + steps) for source in range(first, last)])


def in_blocks(array, dim, count):
    lengths = array.shape
    blocks = array.reshape(*lengths[:dim], count, lengths[dim] // count, *lengths[dim + 1 :])
    return jnp.moveaxis(blocks, dim, 0)


def sum_at_owner(array, axis, dim):
    blocks = in_blocks(array, dim, lax.axis_size(axis))
    arrived = lax.all_to_all(blocks, axis, split_axis=0, concat_axis=0, tiled=True)
    return arrived.astype(jnp.float32).sum(axis=0)


def rms_scale(entry_vectors):
    return lax.rsqrt(jnp.mean(entry_vectors * entry_vectors, axis=-1, keepdims=True) + EPSILON)


def compose(earlier, later):
    return (earlier[0] + later[0], jnp.exp(later[0])[:, :, None] * earlier[1] + later[1])


def per_device(
    tokens,
    norm_gain,
    query_weight,
    forget_weight,
    value_weight,
    outgate_weight,
    pool_in_weight,
    forget_room,
    decay_shift,
    head_gain,
    start_state,
    pool_map,
    pool_scale,
    out_rec_weight,
    out_pool_weight,
):
    widened = gather_directly(tokens, "tp", 2)[0].astype(jnp.float32)
    rescaled_input = (widened * rms_scale(widened) * norm_gain).astype(jnp.bfloat16)
    out_local = jnp.concatenate([out_rec_weight, out_pool_weight], axis=0)
    gathered = gather_turned(
        (query_weight, forget_weight, value_weight, outgate_weight, pool_in_weight, out_local),
        SP_FS,
        (0, 0, 0, 0, 0, 1),
    )
    projected = [
        jnp.dot(rescaled_input, weight, preferred_element_type=jnp.float32).astype(jnp.bfloat16)
        for weight in gathered[:5]
    ]
    length = rescaled_input.shape[0]
    head_count = forget_room.shape[0] // HEAD
    blocks = length // BLOCK
    queries = jax.nn.silu(projected[0].astype(jnp.float32)) * HEAD ** (-0.5)
    keyed = forget_room[None, :] * (1.0 - jax.nn.sigmoid(projected[1].astype(jnp.float32)))
    log_decay = jnp.log1p(-keyed).reshape(length, head_count, HEAD) + decay_shift[0][:, :, None]

    def to_blocks(entry_vectors):
        return entry_vectors.reshape(blocks, BLOCK, head_count, HEAD).transpose(2, 0, 1, 3)

    query_blocks = to_blocks(queries)
    key_blocks = to_blocks(keyed)
    value_blocks = to_blocks(projected[2])
    within = jnp.cumsum(to_blocks(log_decay), axis=2)
    centre = within[:, :, BLOCK // 2 - 1 : BLOCK // 2]
    ending = within[:, :, BLOCK - 1 : BLOCK]
    causal = jnp.tril(jnp.ones((BLOCK, BLOCK), jnp.float32))
    scores = (
        jnp.einsum(
            "hncd,hnsd->hncs",
            (query_blocks * jnp.exp(within - centre)).astype(jnp.bfloat16),
            (key_blocks * jnp.exp(centre - within)).astype(jnp.bfloat16),
            preferred_element_type=jnp.float32,
        )
        * causal
    )
    inside = jnp.einsum(
        "hncs,hnse->hnce",
        scores.astype(jnp.bfloat16),
        value_blocks,
        preferred_element_type=jnp.float32,
    )
    added = jnp.einsum(
        "hncd,hnce->nhde",
        (key_blocks * jnp.exp(ending - within)).astype(jnp.bfloat16),
        value_blocks,
        preferred_element_type=jnp.float32,
    )
    block_decay = ending[:, :, 0, :].transpose(1, 0, 2)

    def advance(memory, inputs):
        decay_piece, added_piece = inputs
        return (jnp.exp(decay_piece)[:, :, None] * memory + added_piece, memory)

    local_state, block_starts = lax.scan(
        advance, jnp.zeros((head_count, HEAD, HEAD), jnp.float32), (block_decay, added)
    )
    decay_before = jnp.cumsum(block_decay, axis=0) - block_decay
    local_decay = jnp.sum(block_decay, axis=0)
    identity = (jnp.zeros_like(local_decay), jnp.zeros_like(local_state))
    prefix_decay, prefix_state = entering_2((local_decay, local_state), SP, compose, identity)
    entering = prefix_state + jnp.exp(prefix_decay)[:, :, None] * start_state[0]
    block_states = block_starts + jnp.exp(decay_before)[:, :, :, None] * entering[None]
    carried = jnp.einsum(
        "hncd,nhde->hnce",
        (query_blocks * jnp.exp(within)).astype(jnp.bfloat16),
        block_states.astype(jnp.bfloat16),
        preferred_element_type=jnp.float32,
    )
    outputs = (inside + carried).transpose(1, 2, 0, 3).reshape(length, head_count, HEAD)
    gating = jax.nn.silu(projected[3].astype(jnp.float32)).reshape(length, head_count, HEAD)
    rec_out = (outputs * rms_scale(outputs) * head_gain * gating).reshape(length, head_count * HEAD)
    rec_out = rec_out.astype(jnp.bfloat16)
    pool_input = projected[4]
    columns = pool_input.shape[1]
    border = shifted(pool_input[length - WIDEST :], SP, 1)
    extended = jnp.concatenate([border, pool_input], axis=0).astype(jnp.float32)
    feature_lane = lax.axis_index("tp") * columns + jnp.arange(columns, dtype=jnp.int32)
    reach = jnp.left_shift(jnp.int32(2), feature_lane // POOL_DIM)
    window_sum = jnp.zeros((length, columns), jnp.float32)
    for offset in range(WIDEST):
        window_sum = window_sum + extended[WIDEST - offset : WIDEST - offset + length] * (
            offset < reach
        ).astype(jnp.float32)
    position = lax.axis_index(SP) * length + jnp.arange(length, dtype=jnp.int32)
    amount = jnp.minimum(position[:, None] + 1, reach[None, :]).astype(jnp.float32)
    pooled = (window_sum / amount - extended[WIDEST:]).astype(jnp.bfloat16)
    group_count = pool_map.shape[0]
    mapped = jnp.einsum(
        "tgc,gcd->tgd",
        pooled.reshape(length, group_count, POOL_DIM),
        pool_map,
        preferred_element_type=jnp.float32,
    )
    pool_out = (mapped.reshape(length, columns) * pool_scale).astype(jnp.bfloat16)
    joined = jnp.concatenate([rec_out, pool_out], axis=1)
    out_whole = gathered[5]
    mixed_rows = sum_at_owner(
        jnp.dot(joined, out_whole, preferred_element_type=jnp.float32).astype(jnp.bfloat16), "tp", 0
    )
    return mixed_rows.astype(jnp.bfloat16)[None]


def solution(mesh):
    finer = Mesh(
        mesh.devices.reshape(8, 4, mesh.shape["fs"], mesh.shape["tp"]), ("sp_0", "sp_1", "fs", "tp")
    )
    placed = (
        P("fs", SP, "tp"),
        P(),
        P(SP_FS, "tp"),
        P(SP_FS, "tp"),
        P(SP_FS, "tp"),
        P(SP_FS, "tp"),
        P(SP_FS, "tp"),
        P("tp"),
        P("fs", SP, "tp"),
        P(),
        P("fs", "tp", None, None),
        P("tp", None, None),
        P("tp"),
        P("tp", SP_FS),
        P("tp", SP_FS),
    )
    return jax.shard_map(
        per_device, mesh=finer, in_specs=placed, out_specs=P("fs", SP_TP, None), check_vma=False
    )
```

profile of v0, /device:TPU:1, one launch (start us, length us, event | category | flops | bytes accessed | tf_op | source)
XLA Modules:
  0.0 264.8 jit_solution(8559160675575011905)
XLA Ops:
  6.5 0.8 constant_dynamic-update-slice_fusion.4
  7.3 0.7 constant_dynamic-update-slice_fusion.3
  8.0 0.7 constant_dynamic-update-slice_fusion.2
  8.7 0.7 constant_dynamic-update-slice_fusion.1
  9.5 0.7 constant_dynamic-update-slice_fusion
  10.2 0.7 fusion.123
  10.9 0.6 copy-done.3
  11.6 0.0 all-gather.6.cloned.1.call-update
  11.6 1.2 copy.43
  12.8 0.0 copy-start.17
  12.8 0.0 copy-start.21
  12.9 1.1 broadcast_in_dim.22
  13.9 6.8 %all-to-all-start = ((bf16[2,1,256,1024]{2,3,1,0:T(8,128)(2,1)}), bf16[2,1,256,1024]{2,3,1,0:T(8,128)(2,1)S(1)}, u32[]{:S(2)}, u32[]{:S(2)}) async-start(bf16[2,1,256,1024]{2,3,1,0:T(8,128)(2,1)} %broadcast_in_dim.22), calls=%async_computation | async-start | bytes 2097152 | tf_op jit(solution)/shard_map/all_to_all | solution.py:19
  20.7 0.6 add_add_fusion
  21.4 0.6 compare_convert_fusion.4
  21.9 0.6 compare_convert_fusion.6
  22.5 0.6 compare_convert_fusion.8
  23.2 0.6 compare_convert_fusion.10
  23.8 0.6 compare_convert_fusion.12
  24.4 0.6 compare_convert_fusion.14
  25.0 0.3 multiply_reduce_fusion
  25.3 0.6 broadcast_bitcast_fusion
  25.9 0.2 bitcast_convert_fusion
  26.1 0.3 fusion.16
  26.4 131.7 %all-gather.6.cloned.1.call-done = bf16[2048,3584]{1,0:T(8,128)(2,1)} async-done(((bf16[16,3584]{1,0:T(8,128)(2,1)}), bf16[2048,3584]{1,0:T(8,128)(2,1)}) %all-gather.6.cloned.1.call-update) | async-done | bytes 14680080 | tf_op jit(solution)/shard_map/all_gather | solution.py:38
  158.1 2.5 negate_log-plus-one_fusion
  160.7 0.2 reshape.375
  160.9 0.2 fusion.89
  161.1 0.5 reduce_window_sum.22
  161.6 7.6 %all-gather.2 = bf16[4,4,128]{2,1,0:T(4,128)(2,1)S(1)} all-gather(bf16[1,4,128]{2,1,0:T(4,128)(2,1)S(1)} %bitcast.212), channel_id=2, replica_groups=mesh['sp_0'=8,'sp_1'=4,'fs'=4,'tp'=2] {'sp_1'}, dimensions={0}, use_global_device_ids=true | all-gather | bytes 5120 | tf_op jit(solution)/shard_map/all_gather | solution.py:58
  169.3 11.1 %all_gather.23 = bf16[8,4,128]{2,1,0:T(4,128)(2,1)S(1)} all-gather(bf16[1,4,128]{2,1,0:T(4,128)(2,1)S(1)} %get-tuple-element.93), channel_id=1, replica_groups=mesh['sp_0'=8,'sp_1'=4,'fs'=4,'tp'=2] {'sp_0'}, dimensions={0}, use_global_device_ids=true | all-gather | bytes 9216 | tf_op jit(solution)/shard_map/all_gather | solution.py:58
  180.4 0.2 reshape.376
  180.6 2.3 fusion.24
  182.9 0.1 reshape.377
  183.0 0.3 fusion.112
  183.3 1.9 while.13
  183.3 0.7 bitcast_dynamic-update-slice_fusion.2
  184.0 0.2 bitcast_add_fusion.2
  184.2 0.7 bitcast_dynamic-update-slice_fusion.2
  185.0 0.2 bitcast_add_fusion.2
  185.2 9.9 %all-gather.1 = bf16[16,128,128]{2,1,0:T(8,128)(2,1)S(1)} all-gather(bf16[4,128,128]{2,1,0:T(8,128)(2,1)S(1)} %convert_element_type.456), channel_id=3, replica_groups=mesh['sp_0'=8,'sp_1'=4,'fs'=4,'tp'=2] {'sp_1'}, dimensions={0}, use_global_device_ids=true | all-gather | bytes 655360 | tf_op jit(solution)/shard_map/all_gather | solution.py:58
  195.1 0.6 exponential_bitcast_fusion.1
  195.7 1.0 fusion.118
  196.7 0.0 all-gather.8.cloned.1.call-update
  196.7 2.7 %multiply_multiply_fusion = f32[256,512]{1,0:T(8,128)S(1)} fusion(bf16[256,2048]{0,1:T(8,128)(2,1)} %copy-done.1, bf16[2048,3584]{1,0:T(8,128)(2,1)} %all-gather.6.cloned.1.call-done), kind=kOutput, calls=%fused_computation.94 | convolution fusion | flops 537788416 | bytes 3670016 | tf_op jit(solution)/shard_map/dot_general | solution.py:125
  199.4 0.2 reshape.374
  199.6 2.6 fusion.30
  202.4 1.3 collective-permute-start
  203.7 1.3 fusion.61
  205.0 0.1 maximum_convert_fusion
  205.2 1.0 fusion.94
  206.3 0.3 fusion.100
  206.5 0.2 copy.68
  206.7 0.2 copy-done.18
  206.9 29.0 %all-gather.8.cloned.1.call-done = bf16[8,4,128,128]{3,2,1,0:T(8,128)(2,1)} async-done(((bf16[1,4,128,128]{3,2,1,0:T(8,128)(2,1)}), bf16[8,4,128,128]{3,2,1,0:T(8,128)(2,1)}) %all-gather.8.cloned.1.call-update) | async-done | bytes 1048592 | tf_op jit(solution)/shard_map/all_gather | solution.py:58
  236.0 2.2 fusion.110
  238.2 1.7 multiply_reduce_fusion.1
  240.0 0.1 copy.67
  240.1 0.2 copy.54
  240.4 0.3 mul.448
  240.7 2.7 %fusion.64 = bf16[256,512]{1,0:T(8,128)(2,1)S(1)} fusion(f32[32,8,4,128]{3,2,1,0:T(4,128)S(1)} %bitcast.202, f32[32,8,4,128]{3,2,1,0:T(4,128)S(1)} %bitcast.205, bf16[256,2048]{0,1:T(8,128)(2,1)} %copy-done.1, bf16[2048,3584]{1,0:T(8,128)(2,1)} %all-gather.6.cloned.1.call-done, f32[512]{0:T(512)S(1)} %copy-done.19), kind=kOutput, calls=%fused_computation.44 | convolution fusion | flops 538181632 | bytes 4458496 | tf_op jit(solution)/shard_map/dot_general | solution.py:125
  243.4 3.5 %fusion.2 = bf16[256,2048]{1,0:T(8,128)(2,1)S(1)} fusion(bf16[2048,3584]{1,0:T(8,128)(2,1)} %all-gather.6.cloned.1.call-done, bf16[256,512]{1,0:T(8,128)(2,1)S(1)} %multiply_convert_fusion, bf16[256,512]{1,0:T(8,128)(2,1)S(1)} %fusion.64), kind=kOutput, calls=%fused_computation.6 | convolution fusion | flops 1075314688 | bytes 5767168 | tf_op jit(solution)/shard_map/dot_general | solution.py:216
  246.9 9.9 %all_to_all.10 = bf16[2,128,2048]{2,1,0:T(8,128)(2,1)S(1)} all-to-all(bf16[2,128,2048]{2,1,0:T(8,128)(2,1)S(1)} %bitcast.200), channel_id=1, replica_groups=mesh['sp_0'=8,'sp_1'=4,'fs'=4,'tp'=2] {'tp'}, dimensions={0} | all-to-all | bytes 2097152 | tf_op jit(solution)/shard_map/all_to_all | solution.py:87
  256.8 1.1 reduce_sum.42
  (69 shorter events, 0.4 us)
Async XLA Ops:
  6.5 199.7 %copy-start = (bf16[2,256,256]{2,1,0:T(8,128)(2,1)S(1)}, bf16[2,256,256]{2,1,0:T(8,128)(2,1)}, u32[]{:S(2)}) copy-start(bf16[2,256,256]{2,1,0:T(8,128)(2,1)} %param.28) | copy-start | bytes 786436
  6.5 151.6 %all-gather.6.cloned.1.call-start = ((), (), s32[]{:S(2)}) async-start(), calls=%async_computation.2 | async-start | bytes 14794752 | tf_op jit(solution)/shard_map/all_gather | solution.py:38
  10.9 0.6 copy-start.3
  12.8 7.9 %copy-start.17 = (f32[1,256,4]{1,2,0:T(4,128)S(1)}, f32[1,256,4]{1,2,0:T(4,128)}, u32[]{:S(2)}) copy-start(f32[1,256,4]{1,2,0:T(4,128)} %param.25) | copy-start | bytes 12292
  12.8 12.5 %copy-start.21 = (f32[128]{0:T(128)S(1)}, f32[128]{0:T(128)}, u32[]{:S(2)}) copy-start(f32[128]{0:T(128)} %param.26) | copy-start | bytes 1540
  13.9 11.1 %all-to-all-start = ((bf16[2,1,256,1024]{2,3,1,0:T(8,128)(2,1)}), bf16[2,1,256,1024]{2,3,1,0:T(8,128)(2,1)S(1)}, u32[]{:S(2)}, u32[]{:S(2)}) async-start(bf16[2,1,256,1024]{2,3,1,0:T(8,128)(2,1)} %broadcast_in_dim.22), calls=%async_computation | async-start | bytes 2097152 | tf_op jit(solution)/shard_map/all_to_all | solution.py:19
  20.7 215.2 %all-gather.8.cloned.1.call-start = ((), (), s32[]{:S(2)}) async-start(), calls=%async_computation.3 | async-start | bytes 1179648 | tf_op jit(solution)/shard_map/all_gather | solution.py:58
  25.0 1.1 copy-start.4
  26.1 132.0 %copy-start.22 = (f32[512]{0:T(512)S(1)}, f32[512]{0:T(512)}, u32[]{:S(2)}) copy-start(f32[512]{0:T(512)} %param.24) | copy-start | bytes 6148
  26.4 154.1 %copy-start.1 = (bf16[256,2048]{0,1:T(8,128)(2,1)}, bf16[256,2048]{0,1:T(8,128)(2,1)S(1)}, u32[]{:S(2)}) copy-start(bf16[256,2048]{0,1:T(8,128)(2,1)S(1)} %fusion.16) | copy-start | bytes 3145732
  202.3 2.8 %copy-start.5 = (f32[512]{0:T(512)S(1)}, f32[512]{0:T(512)}, u32[]{:S(2)}) copy-start(f32[512]{0:T(512)} %get-tuple-element.107) | copy-start | bytes 6148
  202.3 2.8 %copy-start.6 = (f32[512]{0:T(512)S(1)}, f32[512]{0:T(512)}, u32[]{:S(2)}) copy-start(f32[512]{0:T(512)} %get-tuple-element.108) | copy-start | bytes 6148
  202.3 2.8 %copy-start.7 = (f32[512]{0:T(512)S(1)}, f32[512]{0:T(512)}, u32[]{:S(2)}) copy-start(f32[512]{0:T(512)} %get-tuple-element.109) | copy-start | bytes 6148
  202.3 2.8 %copy-start.8 = (f32[512]{0:T(512)S(1)}, f32[512]{0:T(512)}, u32[]{:S(2)}) copy-start(f32[512]{0:T(512)} %get-tuple-element.110) | copy-start | bytes 6148
  202.3 2.8 %copy-start.9 = (f32[512]{0:T(512)S(1)}, f32[512]{0:T(512)}, u32[]{:S(2)}) copy-start(f32[512]{0:T(512)} %get-tuple-element.111) | copy-start | bytes 6148
  202.3 2.8 %copy-start.10 = (f32[512]{0:T(512)S(1)}, f32[512]{0:T(512)}, u32[]{:S(2)}) copy-start(f32[512]{0:T(512)} %get-tuple-element.112) | copy-start | bytes 6148
  202.3 2.8 %copy-start.11 = (f32[512]{0:T(512)S(1)}, f32[512]{0:T(512)}, u32[]{:S(2)}) copy-start(f32[512]{0:T(512)} %get-tuple-element.113) | copy-start | bytes 6148
  202.3 2.8 %copy-start.12 = (f32[512]{0:T(512)S(1)}, f32[512]{0:T(512)}, u32[]{:S(2)}) copy-start(f32[512]{0:T(512)} %get-tuple-element.114) | copy-start | bytes 6148
  202.3 2.8 %copy-start.13 = (f32[512]{0:T(512)S(1)}, f32[512]{0:T(512)}, u32[]{:S(2)}) copy-start(f32[512]{0:T(512)} %get-tuple-element.115) | copy-start | bytes 6148
  202.4 2.8 %copy-start.14 = (f32[512]{0:T(512)S(1)}, f32[512]{0:T(512)}, u32[]{:S(2)}) copy-start(f32[512]{0:T(512)} %get-tuple-element.116) | copy-start | bytes 6148
  202.4 2.8 %copy-start.15 = (f32[512]{0:T(512)S(1)}, f32[512]{0:T(512)}, u32[]{:S(2)}) copy-start(f32[512]{0:T(512)} %get-tuple-element.117) | copy-start | bytes 6148
  202.4 2.8 %copy-start.20 = (s32[256]{0:T(256)S(1)}, s32[256]{0:T(256)}, u32[]{:S(2)}) copy-start(s32[256]{0:T(256)} %add_add_fusion) | copy-start | bytes 3076
  202.4 2.6 collective-permute-start
  206.2 0.7 copy-start.18
  206.2 29.7 %copy-start.2 = (f32[1,4,128,128]{3,2,1,0:T(8,128)S(1)}, f32[1,4,128,128]{3,2,1,0:T(8,128)}, u32[]{:S(2)}) copy-start(f32[1,4,128,128]{3,2,1,0:T(8,128)} %param.27) | copy-start | bytes 786436
  206.2 29.7 %copy-start.16 = (f32[4,128]{1,0:T(4,128)S(1)}, f32[4,128]{1,0:T(4,128)}, u32[]{:S(2)}) copy-start(f32[4,128]{1,0:T(4,128)} %get-tuple-element.78) | copy-start | bytes 6148
  238.2 2.5 copy-start.19
Sparse Core Ops, SparseCore 0:
  11.7 146.3 all-gather.5
  196.8 39.0 all-gather.7
where the time goes:
time: 266 us; the launch traced here: 265 us
  waiting for transfers between devices  161 us (61%)
  blocking collectives  38.6 us (15%)
  matrix products  20 us (8%)
  other arithmetic  14.4 us (5%)
  between operations  14 us (5%)
  local copies, waits for them, and re-layouts  9.02 us (3%)
  starting transfers between devices  8.06 us (3%)
    all_gather x1, waiting for transfers between devices, gather_turned(): filled, at, done = (lax.all_gather(both, axis, axis=0, tiled=True), 0, [])  132 us
    all_gather x1, waiting for transfers between devices, entering_2(): lax.all_gather(part.astype(kind), axis)  29 us
    all_gather x3, blocking collectives, entering_2(): lax.all_gather(part.astype(kind), axis)  28.7 us
    dot_general x5, matrix products, per_device(): jnp.dot(rescaled_input, weight, preferred_element_type=jnp.float32)  12.9 us
    all_to_all x1, blocking collectives, sum_at_owner(): lax.all_to_all(blocks, axis, split_axis=0, concat_axis=0, tiled=True)  9.93 us
    all_to_all x1, starting transfers between devices, from_everyone(): lax.all_to_all(jnp.broadcast_to(array[None], (count, *array.shape)), axis...  6.77 us
  transfers between devices with their start and end apart: 4, of which 2 were waited for; matrix products, arithmetic and copies ran while one was open for 6% of the time, Pallas kernels for 0%

commit v1 on v0

--- a/solution.py
+++ b/solution.py
@@ -14,6 +14,11 @@
 EPSILON = 1e-06
 
 
+def exchange_gather(array, axis, along):
+    outgoing = jnp.stack([array] * lax.axis_size(axis))
+    return jnp.concatenate(lax.all_to_all(outgoing, axis, 0, 0), axis=along)
+
+
 def from_everyone(array, axis):
     count = lax.axis_size(axis)
     return lax.all_to_all(
@@ -35,7 +40,7 @@
 def gather_turned(arrays, axis, dims):
     turned = [jnp.moveaxis(a, dim, 0) for a, dim in zip(arrays, dims)]
     both = jnp.concatenate([t.reshape(len(t), -1) for t in turned], axis=1)
-    filled, at, done = (lax.all_gather(both, axis, axis=0, tiled=True), 0, [])
+    filled, at, done = (exchange_gather(both, axis, 0), 0, [])
     for t, dim in zip(turned, dims):
         slab = filled[:, at : at + t[0].size].reshape(-1, *t.shape[1:])
         done.append(jnp.moveaxis(slab, 0, dim))

time: 266 us -> 467 us (1.76)
  waiting for transfers between devices: 161 us -> 340 us
  starting transfers between devices: 8.06 us -> 22.5 us
    all_to_all x0 -> x1, waiting for transfers between devices: none -> 320 us  [exchange_gather(): return jnp.concatenate(lax.all_to_all(outgoing, axis, 0, 0), axis=along)]
    all_gather x1 -> x0, waiting for transfers between devices: 132 us -> none  [gather_turned(): filled, at, done = (lax.all_gather(both, axis, axis=0, tiled=True), 0, [])]
    all_to_all x0 -> x1, starting transfers between devices: none -> 14.4 us  [exchange_gather(): return jnp.concatenate(lax.all_to_all(outgoing, axis, 0, 0), axis=along)]
    all_gather x1, waiting for transfers between devices: 29 us -> 18 us  [entering_2(): lax.all_gather(part.astype(kind), axis)]
    another operation x0 -> x1, local copies, waits for them, and re-layouts: none -> 6.98 us  [exchange_gather(): outgoing = jnp.stack([array] * lax.axis_size(axis))]
  transfers between devices with their start and end apart: 4 -> 4, of which waited for: 2 -> 3; matrix products, arithmetic and copies ran while one was open for 6% -> 4% of each run, Pallas kernels for 0% -> 0%
where the time goes in v1:
time: 467 us; the launch traced here: 466 us
  waiting for transfers between devices  340 us (73%)
  blocking collectives  42.6 us (9%)
  starting transfers between devices  22.5 us (5%)
  other arithmetic  17.9 us (4%)
  matrix products  17.2 us (4%)
  between operations  14 us (3%)
  local copies, waits for them, and re-layouts  11.8 us (3%)
    all_to_all x1, waiting for transfers between devices, exchange_gather(): return jnp.concatenate(lax.all_to_all(outgoing, axis, 0, 0), axis=along)  320 us
    all_gather x3, blocking collectives, entering_2(): lax.all_gather(part.astype(kind), axis)  32.8 us
    all_gather x1, waiting for transfers between devices, entering_2(): lax.all_gather(part.astype(kind), axis)  18 us
    all_to_all x1, starting transfers between devices, exchange_gather(): return jnp.concatenate(lax.all_to_all(outgoing, axis, 0, 0), axis=along)  14.4 us
    dot_general x5, matrix products, per_device(): jnp.dot(rescaled_input, weight, preferred_element_type=jnp.float32)  12.1 us
    all_to_all x1, blocking collectives, sum_at_owner(): lax.all_to_all(blocks, axis, split_axis=0, concat_axis=0, tiled=True)  9.9 us
  transfers between devices with their start and end apart: 4, of which 3 were waited for; matrix products, arithmetic and copies ran while one was open for 4% of the time, Pallas kernels for 0%

profile of v1, /device:TPU:1, one launch (start us, length us, event | category | flops | bytes accessed | tf_op | source)
XLA Modules:
  0.0 466.1 jit_solution(18025769354872571228)
XLA Ops:
  6.5 1.3 copy.43
  7.9 0.0 copy-start.9
  7.9 0.0 copy-start.10
  7.9 1.1 broadcast_in_dim.22
  9.0 6.8 %all-to-all-start = ((bf16[2,1,256,1024]{2,3,1,0:T(8,128)(2,1)}), bf16[2,1,256,1024]{2,3,1,0:T(8,128)(2,1)S(1)}, u32[]{:S(2)}, u32[]{:S(2)}) async-start(bf16[2,1,256,1024]{2,3,1,0:T(8,128)(2,1)} %broadcast_in_dim.22), calls=%async_computation | async-start | bytes 2097152 | tf_op jit(solution)/shard_map/all_to_all | solution.py:24
  15.9 1.6 all-to-all-done
  17.5 7.0 %stack.2 = bf16[128,16,3584]{2,1,0:T(8,128)(2,1)} broadcast(bf16[16,3584]{1,0:T(8,128)(2,1)S(1)} %fusion.123), dimensions={1,2} | broadcast | bytes 14794752 | tf_op jit(solution)/shard_map/stack | solution.py:18
  24.5 14.4 %all-to-all-start.1 = ((bf16[128,16,3584]{2,1,0:T(8,128)(2,1)}), bf16[128,16,3584]{2,1,0:T(8,128)(2,1)}, u32[]{:S(2)}, u32[]{:S(2)}) async-start(bf16[128,16,3584]{2,1,0:T(8,128)(2,1)} %stack.2), calls=%async_computation.1 | async-start | bytes 29360128 | tf_op jit(solution)/shard_map/all_to_all | solution.py:19
  38.9 0.0 all-gather.5.cloned.1.call-start
  39.0 0.5 add_add_fusion
  39.6 0.6 fusion.147
  40.2 0.6 compare_convert_fusion
  40.8 0.6 compare_convert_fusion.2
  41.3 0.6 compare_convert_fusion.4
  41.9 0.6 compare_convert_fusion.6
  42.5 0.6 compare_convert_fusion.8
  43.1 0.6 compare_convert_fusion.10
  43.7 0.6 compare_convert_fusion.12
  44.3 0.6 compare_convert_fusion.14
  45.0 0.3 multiply_reduce_fusion
  45.3 0.6 broadcast_bitcast_fusion
  45.9 0.2 bitcast_convert_fusion
  46.0 0.3 fusion.16
  46.4 320.3 %all-to-all-done.1 = bf16[128,16,3584]{2,1,0:T(8,128)(2,1)} async-done(((bf16[128,16,3584]{2,1,0:T(8,128)(2,1)}), bf16[128,16,3584]{2,1,0:T(8,128)(2,1)}, u32[]{:S(2)}, u32[]{:S(2)}) %all-to-all-start.1) | async-done | bytes 14680096 | tf_op jit(solution)/shard_map/all_to_all | solution.py:19
  366.7 2.3 fusion.30
  369.1 2.5 multiply_multiply_fusion
  371.6 2.3 fusion.24
  373.9 1.3 collective-permute-start
  375.2 2.5 negate_log-plus-one_fusion
  377.8 0.2 reshape.381
  378.0 0.2 reshape.380
  378.2 0.2 reshape.382
  378.4 0.1 reshape.383
  378.4 0.2 fusion.89
  378.6 0.5 reduce_window_sum.22
  379.2 0.3 fusion.112
  379.5 1.9 while.13
  379.5 0.7 bitcast_dynamic-update-slice_fusion.2
  380.2 0.2 bitcast_add_fusion.2
  380.4 0.7 bitcast_dynamic-update-slice_fusion.2
  381.2 0.2 bitcast_add_fusion.2
  381.4 7.5 %all-gather.2 = bf16[4,4,128]{2,1,0:T(4,128)(2,1)S(1)} all-gather(bf16[1,4,128]{2,1,0:T(4,128)(2,1)S(1)} %bitcast.212), channel_id=2, replica_groups=mesh['sp_0'=8,'sp_1'=4,'fs'=4,'tp'=2] {'sp_1'}, dimensions={0}, use_global_device_ids=true | all-gather | bytes 5120 | tf_op jit(solution)/shard_map/all_gather | solution.py:63
  388.9 10.4 %all-gather.1 = bf16[16,128,128]{2,1,0:T(8,128)(2,1)S(1)} all-gather(bf16[4,128,128]{2,1,0:T(8,128)(2,1)S(1)} %convert_element_type.456), channel_id=3, replica_groups=mesh['sp_0'=8,'sp_1'=4,'fs'=4,'tp'=2] {'sp_1'}, dimensions={0}, use_global_device_ids=true | all-gather | bytes 655360 | tf_op jit(solution)/shard_map/all_gather | solution.py:63
  399.4 0.6 exponential_bitcast_fusion.1
  400.0 1.0 fusion.118
  401.0 0.0 all-gather.5.cloned.1.call-update
  401.0 14.8 %all_gather.19 = bf16[8,4,128]{2,1,0:T(4,128)(2,1)S(1)} all-gather(bf16[1,4,128]{2,1,0:T(4,128)(2,1)S(1)} %get-tuple-element.93), channel_id=1, replica_groups=mesh['sp_0'=8,'sp_1'=4,'fs'=4,'tp'=2] {'sp_0'}, dimensions={0}, use_global_device_ids=true | all-gather | bytes 9216 | tf_op jit(solution)/shard_map/all_gather | solution.py:63
  415.8 0.5 fusion.61
  416.3 1.0 maximum_convert_fusion
  417.3 1.8 fusion.94
  419.1 0.3 fusion.100
  419.4 0.2 copy.68
  419.6 0.2 copy-done.16
  419.8 0.8 multiply_convert_fusion
  420.5 18.0 %all-gather.5.cloned.1.call-done = bf16[8,4,128,128]{3,2,1,0:T(8,128)(2,1)} async-done(((bf16[1,4,128,128]{3,2,1,0:T(8,128)(2,1)}), bf16[8,4,128,128]{3,2,1,0:T(8,128)(2,1)}) %all-gather.5.cloned.1.call-update) | async-done | bytes 1048592 | tf_op jit(solution)/shard_map/all_gather | solution.py:63
  438.6 2.4 fusion.110
  441.0 0.5 multiply_reduce_fusion.1
  441.5 0.1 copy.67
  441.6 0.2 copy.54
  441.9 0.3 mul.448
  442.3 2.4 fusion.64
  444.7 3.5 fusion.2
  448.2 9.9 %all_to_all.15 = bf16[2,128,2048]{2,1,0:T(8,128)(2,1)S(1)} all-to-all(bf16[2,128,2048]{2,1,0:T(8,128)(2,1)S(1)} %bitcast.201), channel_id=1, replica_groups=mesh['sp_0'=8,'sp_1'=4,'fs'=4,'tp'=2] {'tp'}, dimensions={0} | all-to-all | bytes 2097152 | tf_op jit(solution)/shard_map/all_to_all | solution.py:92
  458.1 1.1 reduce_sum.42
  (63 shorter events, 0.3 us)
Async XLA Ops:
  6.5 412.6 %copy-start = (bf16[2,256,256]{2,1,0:T(8,128)(2,1)S(1)}, bf16[2,256,256]{2,1,0:T(8,128)(2,1)}, u32[]{:S(2)}) copy-start(bf16[2,256,256]{2,1,0:T(8,128)(2,1)} %param.28) | copy-start | bytes 786436
  6.5 9.2 %copy-start.6 = (bf16[16,512]{1,0:T(8,128)(2,1)S(1)}, bf16[16,512]{1,0:T(8,128)(2,1)}, u32[]{:S(2)}) copy-start(bf16[16,512]{1,0:T(8,128)(2,1)} %param.19) | copy-start | bytes 49156
  7.8 7.9 %copy-start.7 = (bf16[16,512]{1,0:T(8,128)(2,1)S(1)}, bf16[16,512]{1,0:T(8,128)(2,1)}, u32[]{:S(2)}) copy-start(bf16[16,512]{1,0:T(8,128)(2,1)} %param.20) | copy-start | bytes 49156
  7.9 7.9 %copy-start.8 = (bf16[16,512]{1,0:T(8,128)(2,1)S(1)}, bf16[16,512]{1,0:T(8,128)(2,1)}, u32[]{:S(2)}) copy-start(bf16[16,512]{1,0:T(8,128)(2,1)} %param.21) | copy-start | bytes 49156
  7.9 7.9 %copy-start.9 = (bf16[16,512]{1,0:T(8,128)(2,1)S(1)}, bf16[16,512]{1,0:T(8,128)(2,1)}, u32[]{:S(2)}) copy-start(bf16[16,512]{1,0:T(8,128)(2,1)} %param.22) | copy-start | bytes 49156
  7.9 7.9 %copy-start.10 = (bf16[16,512]{1,0:T(8,128)(2,1)S(1)}, bf16[16,512]{1,0:T(8,128)(2,1)}, u32[]{:S(2)}) copy-start(bf16[16,512]{1,0:T(8,128)(2,1)} %param.23) | copy-start | bytes 49156
  7.9 8.0 %copy-start.11 = (bf16[512,16]{0,1:T(8,128)(2,1)S(1)}, bf16[512,16]{0,1:T(8,128)(2,1)}, u32[]{:S(2)}) copy-start(bf16[512,16]{0,1:T(8,128)(2,1)} %param.31) | copy-start | bytes 49156
  7.9 8.0 %copy-start.12 = (bf16[512,16]{0,1:T(8,128)(2,1)S(1)}, bf16[512,16]{0,1:T(8,128)(2,1)}, u32[]{:S(2)}) copy-start(bf16[512,16]{0,1:T(8,128)(2,1)} %param.30) | copy-start | bytes 49156
  9.0 8.5 %all-to-all-start = ((bf16[2,1,256,1024]{2,3,1,0:T(8,128)(2,1)}), bf16[2,1,256,1024]{2,3,1,0:T(8,128)(2,1)S(1)}, u32[]{:S(2)}, u32[]{:S(2)}) async-start(bf16[2,1,256,1024]{2,3,1,0:T(8,128)(2,1)} %broadcast_in_dim.22), calls=%async_computation | async-start | bytes 2097152 | tf_op jit(solution)/shard_map/all_to_all | solution.py:24
  24.5 14.5 %copy-start.15 = (f32[1,256,4]{1,2,0:T(4,128)S(1)}, f32[1,256,4]{1,2,0:T(4,128)}, u32[]{:S(2)}) copy-start(f32[1,256,4]{1,2,0:T(4,128)} %param.25) | copy-start | bytes 12292
  24.5 20.8 %copy-start.18 = (f32[128]{0:T(128)S(1)}, f32[128]{0:T(128)}, u32[]{:S(2)}) copy-start(f32[128]{0:T(128)} %param.26) | copy-start | bytes 1540
  24.5 342.2 %all-to-all-start.1 = ((bf16[128,16,3584]{2,1,0:T(8,128)(2,1)}), bf16[128,16,3584]{2,1,0:T(8,128)(2,1)}, u32[]{:S(2)}, u32[]{:S(2)}) async-start(bf16[128,16,3584]{2,1,0:T(8,128)(2,1)} %stack.2), calls=%async_computation.1 | async-start | bytes 29360128 | tf_op jit(solution)/shard_map/all_to_all | solution.py:19
  38.9 399.6 %all-gather.5.cloned.1.call-start = ((), (), s32[]{:S(2)}) async-start(), calls=%async_computation.3 | async-start | bytes 1179648 | tf_op jit(solution)/shard_map/all_gather | solution.py:63
  44.9 1.1 copy-start.13
  46.4 328.8 %copy-start.1 = (bf16[256,2048]{0,1:T(8,128)(2,1)}, bf16[256,2048]{0,1:T(8,128)(2,1)S(1)}, u32[]{:S(2)}) copy-start(bf16[256,2048]{0,1:T(8,128)(2,1)S(1)} %fusion.16) | copy-start | bytes 3145732
  369.0 4.8 %copy-start.4 = (bf16[256,512]{1,0:T(8,128)(2,1)}, bf16[256,512]{1,0:T(8,128)(2,1)S(1)}, u32[]{:S(2)}) copy-start(bf16[256,512]{1,0:T(8,128)(2,1)S(1)} %fusion.30) | copy-start | bytes 786436
  371.5 3.7 copy-start.19
  373.9 42.4 %collective-permute-start = (bf16[16,512]{1,0:T(8,128)(2,1)S(1)}, bf16[16,512]{1,0:T(8,128)(2,1)S(1)}, u32[]{:S(2)}, u32[]{:S(2)}) collective-permute-start(bf16[16,512]{1,0:T(8,128)(2,1)S(1)} %slice.240), channel_id=1, source_target_pairs={{0,8},{8,16},{16,24},{24,32},{32,40},{40,48},{48,56},{56,64},{64,7... | collective-permute-start | bytes 49160 | tf_op jit(solution)/shard_map/ppermute | solution.py:81
  419.1 0.7 copy-start.16
  419.1 19.5 %copy-start.14 = (f32[4,128]{1,0:T(4,128)S(1)}, f32[4,128]{1,0:T(4,128)}, u32[]{:S(2)}) copy-start(f32[4,128]{1,0:T(4,128)} %get-tuple-element.78) | copy-start | bytes 6148
  438.5 2.4 copy-start.3
  440.9 1.3 copy-start.2
  440.9 1.3 copy-start.17
  442.2 2.5 copy-start.5
Sparse Core Ops, SparseCore 0:
  401.1 37.3 all-gather.4
